TPU v7x, 32 devices: a whole 2x2x4 slice. The times are simulated.
32 devices in a mesh: dp: 4 (over y, x), kv: 4 (over z), tp: 2 (over core).
Axes of the slice: x: 2, y: 2, z: 4, core: 2. Of those that a mesh axis runs over, the one named last changes fastest.
Arguments:
- tokens: bfloat16 [4, 16, 2048], P('dp', None, 'kv'), may hold values from -18 to 18, as said below
- norm_gain: float32 [2048], P('kv'), may hold values from 0.1 to 1.9
- w_query: bfloat16 [2048, 3072], P('kv', 'tp'), may hold values from -0.125 to 0.125
- w_key: bfloat16 [2048, 3072], P('kv', 'tp'), may hold values from -0.125 to 0.125
- w_value: bfloat16 [2048, 3072], P('kv', 'tp'), may hold values from -0.125 to 0.125
- w_gate: bfloat16 [2048, 3072], P('kv', 'tp'), may hold values from -0.125 to 0.125
- w_out: bfloat16 [3072, 2048], P('tp', 'kv'), may hold values from -0.109375 to 0.109375
- head_bias: float32 [24], P('tp'), may hold values from -14 to -2
- cache_keys: bfloat16 [4, 2048, 24, 128], P('dp', 'kv', 'tp'), may hold values from -18 to 18, as said below
- cache_values: bfloat16 [4, 2048, 24, 128], P('dp', 'kv', 'tp'), may hold values from -6 to 6
- prefix_len: int32 [4], P('dp'), may hold values from 1536 to 2028
- accepted: int32 [4], P('dp'), may hold values from 1 to 4
- parent: int32 [4, 16], P('dp'), may hold values from -1 to 14, as said below
Outputs:
- mixed: bfloat16 [4, 16, 2048], P('dp', None, 'kv')
- keys_next: bfloat16 [4, 2048, 24, 128], P('dp', 'kv', 'tp')
- values_next: bfloat16 [4, 2048, 24, 128], P('dp', 'kv', 'tp')
Inputs may be any that keep to these rules, and one draw needn't show every extreme that they name: `tokens`: entries of order one. `cache_keys`: entries of order one. parent of proposal 0 is -1; for p of 1 or more, parent[p] lies in max(p - 3, 0) to p - 1.
All inputs are finite; a program needn't handle non-finite values.
Results may differ from a plain program's by a relative error of at most 0.012.
Values may be sent and summed in bfloat16 or wider, within the bound.
A program may use at most 64 MiB of HBM per device.

v0:
```python
import jax
import jax.numpy as jnp
from jax import lax
from jax.sharding import PartitionSpec as P

D = 2048
HEAD = 128
EPS = 1e-06


def ancestry(parent):
    count = parent.shape[-1]
    places = jnp.arange(count, dtype=jnp.int32)
    reach = (parent[:, :, None] == places[None, None, :]).astype(jnp.float32)
    for repeat in range(count.bit_length()):
        reach = jnp.minimum(
            reach + jnp.einsum("spj,sjk->spk", reach, reach, precision=lax.Precision.HIGHEST), 1.0
        )
    return reach > 0.5


def after_table(count):
    places = jnp.arange(count, dtype=jnp.int32)
    return (places[:, None] > places[None, :]).astype(jnp.float32)


def sum_after(values):
    table = after_table(values.shape[-1])
    return jnp.einsum("shpk,kc->shpc", values, table, precision=lax.Precision.HIGHEST)


def local(
    tokens,
    norm_gain,
    w_query,
    w_key,
    w_value,
    w_gate,
    w_out,
    head_bias,
    cache_keys,
    cache_values,
    prefix_len,
    accepted,
    parent,
):
    seqs, props, columns = tokens.shape
    width = w_query.shape[1]
    heads = width // HEAD
    flat = tokens.astype(jnp.float32).reshape(seqs * props, columns)
    square_part = jnp.sum(flat * flat, axis=1)
    scaled = (flat * norm_gain).astype(jnp.bfloat16)
    partial_value = jnp.concatenate(
        [
            jnp.dot(scaled, weight, preferred_element_type=jnp.float32)
            for weight in (w_query, w_key, w_value, w_gate)
        ],
        axis=1,
    )
    squares = lax.psum(square_part, "kv")
    share = lax.psum_scatter(partial_value, "kv", scatter_dimension=1, tiled=True)
    rscale = lax.rsqrt(squares / D + EPS)
    projected = lax.all_gather(
        (share * rscale[:, None]).astype(jnp.bfloat16), "kv", axis=1, tiled=True
    )
    shaped = projected.reshape(seqs, props, 4, heads, HEAD)
    query = shaped[:, :, 0]
    key_new = shaped[:, :, 1]
    value_new = shaped[:, :, 2]
    gate = projected[:, 3 * width :].astype(jnp.float32)
    factor = HEAD ** (-0.5)
    bias_col = head_bias[None, :, None, None]
    ctx_dev = cache_keys.shape[1]
    places = lax.axis_index("kv") * ctx_dev + jnp.arange(ctx_dev, dtype=jnp.int32)
    valid = prefix_len + accepted
    live = (places[None, :] < valid[:, None])[:, None, None, :]
    scores = (
        jnp.einsum("sphd,schd->shpc", query, cache_keys, preferred_element_type=jnp.float32)
        * factor
        + bias_col
    )
    keep_log = jnp.where(live, jax.nn.log_sigmoid(-scores), 0.0)
    shard_rest = jnp.sum(keep_log, axis=3)
    family = ancestry(parent)[:, None]
    tree_scores = (
        jnp.einsum("sphd,sjhd->shpj", query, key_new, preferred_element_type=jnp.float32) * factor
        + bias_col
    )
    tree_keep = jnp.where(family, jax.nn.log_sigmoid(-tree_scores), 0.0)
    tail = jnp.sum(tree_keep, axis=3)
    every = lax.all_gather(shard_rest[None], "kv", axis=0, tiled=True)
    after = jnp.arange(every.shape[0], dtype=jnp.int32) > lax.axis_index("kv")
    beyond = jnp.sum(jnp.where(after[:, None, None, None], every, 0.0), axis=0)
    later_cache = sum_after(keep_log) + (beyond + tail)[..., None]
    cache_weight = jnp.where(live, jnp.exp(jax.nn.log_sigmoid(scores) + later_cache), 0.0).astype(
        jnp.bfloat16
    )
    later_tree = sum_after(tree_keep)
    tree_weight = jnp.where(
        family, jnp.exp(jax.nn.log_sigmoid(tree_scores) + later_tree), 0.0
    ).astype(jnp.bfloat16)
    local_sum = jnp.einsum(
        "shpc,schd->sphd", cache_weight, cache_values, preferred_element_type=jnp.float32
    )
    attended = lax.psum(local_sum, "kv")
    attended = attended + jnp.einsum(
        "shpj,sjhd->sphd", tree_weight, value_new, preferred_element_type=jnp.float32
    )
    mixin = (attended.reshape(seqs * props, width) * jax.nn.silu(gate)).astype(jnp.bfloat16)
    part_out = jnp.dot(mixin, w_out, preferred_element_type=jnp.float32).astype(jnp.bfloat16)
    part_out = lax.optimization_barrier(part_out).astype(jnp.float32)
    mixed = lax.psum(part_out.astype(jnp.bfloat16), "tp").reshape(seqs, props, w_out.shape[1])
    relative = places[None, :] - valid[:, None]
    picker = (relative[:, :, None] == jnp.arange(props, dtype=jnp.int32)[None, None, :]).astype(
        jnp.bfloat16
    )
    inside = ((relative >= 0) & (relative < props))[:, :, None, None]
    placed_keys = jnp.einsum(
        "scp,sphd->schd", picker, key_new, preferred_element_type=jnp.float32
    ).astype(jnp.bfloat16)
    placed_values = jnp.einsum(
        "scp,sphd->schd", picker, value_new, preferred_element_type=jnp.float32
    ).astype(jnp.bfloat16)
    keys_next = jnp.where(inside, placed_keys, cache_keys)
    values_next = jnp.where(inside, placed_values, cache_values)
    return (mixed, keys_next, values_next)


def solution(mesh):
    return jax.shard_map(
        local,
        mesh=mesh,
        in_specs=(
            P("dp", None, "kv"),
            P("kv"),
            P("kv", "tp"),
            P("kv", "tp"),
            P("kv", "tp"),
            P("kv", "tp"),
            P("tp", "kv"),
            P("tp"),
            P("dp", "kv", "tp", None),
            P("dp", "kv", "tp", None),
            P("dp"),
            P("dp"),
            P("dp", None),
        ),
        out_specs=(P("dp", None, "kv"), P("dp", "kv", "tp", None), P("dp", "kv", "tp", None)),
        check_vma=False,
    )
```

profile of v0, /device:TPU:0, one launch (start us, length us, event | category | flops | bytes accessed | tf_op | source)
XLA Modules:
  0.0 114.4 jit_solution(16729290940814623827)
XLA Ops:
  7.3 1.3 %copy-done = bf16[512,1536]{1,0:T(8,128)(2,1)S(1)} copy-done((bf16[512,1536]{1,0:T(8,128)(2,1)S(1)}, bf16[512,1536]{1,0:T(8,128)(2,1)}, u32[]{:S(2)}) %copy-start) | copy-done | bytes 1572888
  8.6 1.1 fusion.70
  9.8 0.3 fusion.68
  10.1 0.3 fusion.66
  10.4 0.8 copy-done.6
  11.6 0.8 pad_maximum_fusion
  14.7 13.6 %psum.21 = f32[16]{0:T(128)S(1)} all-reduce(f32[16]{0:T(128)S(1)} %fusion.52), channel_id=1, replica_groups=mesh['dp'=4,'kv'=4,'tp'=2] {'kv'}, use_global_device_ids=true, to_apply=%region_2.0 | all-reduce | flops 16 | bytes 128 | tf_op jit(solution)/shard_map/psum | solution.py:60
  28.4 7.6 %reduce-scatter.2.cloned.1.call-done = f32[16,1536]{1,0:T(8,128)} async-done(((f32[16,6144]{1,0:T(8,128)}), f32[16,1536]{1,0:T(8,128)}) %reduce-scatter.2.cloned.1.call-update) | async-done | bytes 98320 | tf_op jit(solution)/shard_map/reduce_scatter | solution.py:61
  36.0 1.0 multiply_convert_fusion
  37.0 13.6 %all_gather.6 = bf16[16,6144]{1,0:T(8,128)(2,1)S(1)} all-gather(bf16[16,1536]{1,0:T(8,128)(2,1)S(1)} %multiply_convert_fusion), channel_id=1, replica_groups=mesh['dp'=4,'kv'=4,'tp'=2] {'kv'}, dimensions={1}, use_global_device_ids=true | all-gather | bytes 245760 | tf_op jit(solution)/shard_map/all_gather | solution.py:63
  50.6 0.9 reshape.356
  51.4 0.9 fusion.80
  52.6 0.5 fusion.32
  53.1 0.3 fusion.31
  53.4 13.2 %all-gather.1 = f32[4,12,16]{2,1,0:T(8,128)S(1)} all-gather(f32[1,12,16]{2,1,0:T(8,128)S(1)} %bitcast.103), channel_id=2, replica_groups=mesh['dp'=4,'kv'=4,'tp'=2] {'kv'}, dimensions={0}, use_global_device_ids=true | all-gather | bytes 3840 | tf_op jit(solution)/shard_map/all_gather | solution.py:91
  66.8 0.9 fusion.13
  67.7 0.5 copy-done.2
  68.2 1.0 fusion.14
  69.2 1.8 %bitcast_select_fusion.1 = bf16[1,512,12,128]{3,1,2,0:T(8,128)(2,1)} fusion(bf16[1,512,12,128]{3,1,2,0:T(8,128)(2,1)S(1)} %copy-done.1, pred[512]{0:T(512)(128)(4,1)S(1)} %compare_and_fusion, bf16[1,16,1,12,128]{4,3,2,1,0:T(8,128)(2,1)S(1)} %get-tuple-element.4, s32[512]{0:T(512)S(1)} %fusion.73), kind=kOutput, calls=%fused_computation.3 | convolution fusion | flops 26746880 | bytes 3197440 | tf_op jit(solution)/shard_map/scp,sphd->schd/dot_general | solution.py:118
  70.9 1.8 %bitcast_select_fusion = bf16[1,512,12,128]{3,1,2,0:T(8,128)(2,1)} fusion(bf16[1,512,12,128]{3,1,2,0:T(8,128)(2,1)S(1)} %copy-done.3, pred[512]{0:T(512)(128)(4,1)S(1)} %compare_and_fusion, bf16[1,16,1,12,128]{4,3,2,1,0:T(8,128)(2,1)S(1)} %get-tuple-element.3, s32[512]{0:T(512)S(1)} %fusion.73), kind=kOutput, calls=%fused_computation.2 | convolution fusion | flops 26746880 | bytes 3197440 | tf_op jit(solution)/shard_map/scp,sphd->schd/dot_general | solution.py:121
  73.0 29.2 %all-reduce.2.cloned.1.call-done = f32[1,16,12,128]{3,1,2,0:T(8,128)} async-done(((f32[1,16,12,128]{3,1,2,0:T(8,128)}), f32[1,16,12,128]{3,1,2,0:T(8,128)}) %all-reduce.2.cloned.1.call-update) | async-done | bytes 98320 | tf_op jit(solution)/shard_map/psum | solution.py:105
  102.2 1.1 fusion.17
  103.3 0.3 convolution_convert_fusion.2
  103.6 4.0 %psum.23 = bf16[1,16,512]{2,1,0:T(8,128)(2,1)} all-reduce(bf16[1,16,512]{2,1,0:T(8,128)(2,1)S(1)} %bitcast.102), channel_id=1, replica_groups=mesh['dp'=4,'kv'=4,'tp'=2] {'tp'}, use_global_device_ids=true, to_apply=%region_7.8 | all-reduce | flops 8192 | bytes 32768 | tf_op jit(solution)/shard_map/psum | solution.py:112
  (48 shorter events, 2.2 us)
Async XLA Ops:
  7.2 1.4 %copy-start = (bf16[512,1536]{1,0:T(8,128)(2,1)S(1)}, bf16[512,1536]{1,0:T(8,128)(2,1)}, u32[]{:S(2)}) copy-start(bf16[512,1536]{1,0:T(8,128)(2,1)} %param.15) | copy-start | bytes 4718596
  7.2 2.5 %copy-start.8 = (bf16[1,16,512]{2,1,0:T(8,128)(2,1)S(1)}, bf16[1,16,512]{2,1,0:T(8,128)(2,1)}, u32[]{:S(2)}) copy-start(bf16[1,16,512]{2,1,0:T(8,128)(2,1)} %param.13) | copy-start | bytes 49156
  7.2 2.5 %copy-start.11 = (f32[512]{0:T(512)S(1)}, f32[512]{0:T(512)}, u32[]{:S(2)}) copy-start(f32[512]{0:T(512)} %param.14) | copy-start | bytes 6148
  7.2 2.5 %copy-start.4 = (bf16[512,1536]{1,0:T(8,128)(2,1)S(1)}, bf16[512,1536]{1,0:T(8,128)(2,1)}, u32[]{:S(2)}) copy-start(bf16[512,1536]{1,0:T(8,128)(2,1)} %param.16) | copy-start | bytes 4718596
  7.2 28.8 %reduce-scatter.2.cloned.1.call-start = ((), (), s32[]{:S(2)}) async-start(), calls=%async_computation.1 | async-start | bytes 491520 | tf_op jit(solution)/shard_map/reduce_scatter | solution.py:61
  8.6 1.6 %copy-start.5 = (bf16[512,1536]{1,0:T(8,128)(2,1)S(1)}, bf16[512,1536]{1,0:T(8,128)(2,1)}, u32[]{:S(2)}) copy-start(bf16[512,1536]{1,0:T(8,128)(2,1)} %param.17) | copy-start | bytes 4718596
  9.8 1.5 %copy-start.6 = (bf16[512,1536]{1,0:T(8,128)(2,1)S(1)}, bf16[512,1536]{1,0:T(8,128)(2,1)}, u32[]{:S(2)}) copy-start(bf16[512,1536]{1,0:T(8,128)(2,1)} %param.18) | copy-start | bytes 4718596
  11.3 1.2 %copy-start.13 = (s32[1,16]{1,0:T(1,128)S(1)}, s32[1,16]{1,0:T(1,128)}, u32[]{:S(2)}) copy-start(s32[1,16]{1,0:T(1,128)} %param.25) | copy-start | bytes 196
  11.6 40.8 %copy-start.12 = (f32[12]{0:T(128)S(1)}, f32[12]{0:T(128)}, u32[]{:S(2)}) copy-start(f32[12]{0:T(128)} %param.20) | copy-start | bytes 148
  11.6 41.0 %copy-start.1 = (bf16[1,512,12,128]{3,1,2,0:T(8,128)(2,1)S(1)}, bf16[1,512,12,128]{3,1,2,0:T(8,128)(2,1)}, u32[]{:S(2)}) copy-start(bf16[1,512,12,128]{3,1,2,0:T(8,128)(2,1)} %param.21) | copy-start | bytes 4718596
  12.4 89.8 %all-reduce.2.cloned.1.call-start = ((), (), s32[]{:S(2)}) async-start(), calls=%async_computation.2 | async-start | bytes 196608 | tf_op jit(solution)/shard_map/psum | solution.py:105
  52.5 15.1 %copy-start.9 = (f32[12,16,16]{1,2,0:T(8,128)}, f32[12,16,16]{1,2,0:T(8,128)S(1)}, u32[]{:S(2)}) copy-start(f32[12,16,16]{1,2,0:T(8,128)S(1)} %get-tuple-element.9) | copy-start | bytes 36868
  66.7 1.4 %copy-start.2 = (bf16[1,512,12,128]{3,1,2,0:T(8,128)(2,1)S(1)}, bf16[1,512,12,128]{3,1,2,0:T(8,128)(2,1)}, u32[]{:S(2)}) copy-start(bf16[1,512,12,128]{3,1,2,0:T(8,128)(2,1)} %param.22) | copy-start | bytes 4718596
  69.1 1.8 %copy-start.3 = (bf16[1,512,12,128]{3,1,2,0:T(8,128)(2,1)S(1)}, bf16[1,512,12,128]{3,1,2,0:T(8,128)(2,1)}, u32[]{:S(2)}) copy-start(bf16[1,512,12,128]{3,1,2,0:T(8,128)(2,1)} %param.22) | copy-start | bytes 4718596
  70.9 1.8 %copy-start.10 = (f32[12,16,16]{1,2,0:T(8,128)S(1)}, f32[12,16,16]{1,2,0:T(8,128)}, u32[]{:S(2)}) copy-start(f32[12,16,16]{1,2,0:T(8,128)} %copy-done.9) | copy-start | bytes 36868
  70.9 32.4 %copy-start.7 = (bf16[1536,512]{1,0:T(8,128)(2,1)S(1)}, bf16[1536,512]{1,0:T(8,128)(2,1)}, u32[]{:S(2)}) copy-start(bf16[1536,512]{1,0:T(8,128)(2,1)} %param.19) | copy-start | bytes 4718596
Sparse Core Ops, SparseCore 0:
  12.5 23.4 reduce-scatter.1
  69.3 32.8 all-reduce.1
where the time goes:
time: 115 us; the launch traced here: 114 us
  blocking collectives  44.4 us (39%)
  waiting for transfers between devices  36.8 us (32%)
  between operations  15.6 us (14%)
  matrix products  10.6 us (9%)
  local copies, waits for them, and re-layouts  4.63 us (4%)
  other arithmetic  2.38 us (2%)
    psum x1, waiting for transfers between devices, local(): attended = lax.psum(local_sum, 'kv')  29.2 us
    psum x1, blocking collectives, local(): squares = lax.psum(square_part, 'kv')  13.6 us
    all_gather x1, blocking collectives, local(): lax.all_gather((share * rscale[:, None]).astype(jnp.bfloat16), 'kv', axis...  13.6 us
    all_gather x1, blocking collectives, local(): every = lax.all_gather(shard_rest[None], 'kv', axis=0, tiled=True)  13.2 us
    reduce_scatter x1, waiting for transfers between devices, local(): lax.psum_scatter(partial_value, 'kv', scatter_dimension=1, tiled=True)  7.6 us
    psum x1, blocking collectives, local(): lax.psum(part_out.astype(jnp.bfloat16), 'tp')  3.96 us
    unnamed x28, local copies, waits for them, and re-layouts  2.74 us
  transfers between devices with their start and end apart: 2, of which 2 were waited for; matrix products, arithmetic and copies ran while one was open for 4% of the time, Pallas kernels for 0%

commit v1 on v0

--- a/solution.py
+++ b/solution.py
@@ -60,8 +60,8 @@
     squares = lax.psum(square_part, "kv")
     share = lax.psum_scatter(partial_value, "kv", scatter_dimension=1, tiled=True)
     rscale = lax.rsqrt(squares / D + EPS)
-    projected = lax.all_gather(
-        (share * rscale[:, None]).astype(jnp.bfloat16), "kv", axis=1, tiled=True
+    projected = jnp.concatenate(
+        lax.all_gather((share * rscale[:, None]).astype(jnp.bfloat16), "kv"), axis=1
     )
     shaped = projected.reshape(seqs, props, 4, heads, HEAD)
     query = shaped[:, :, 0]

time: 115 us -> 116 us (level)
    unnamed x28 -> x29, local copies, waits for them, and re-layouts: 2.74 us -> 3.44 us
  transfers between devices with their start and end apart: 2 -> 2, of which waited for: 2 -> 2; matrix products, arithmetic and copies ran while one was open for 4% -> 5% of each run, Pallas kernels for 0% -> 0%
where the time goes in v1:
time: 116 us; the launch traced here: 115 us
  blocking collectives  44.4 us (38%)
  waiting for transfers between devices  36.1 us (31%)
  between operations  15.6 us (13%)
  matrix products  11.4 us (10%)
  local copies, waits for them, and re-layouts  5.47 us (5%)
  other arithmetic  2.38 us (2%)
    psum x1, waiting for transfers between devices, local(): attended = lax.psum(local_sum, 'kv')  28.5 us
    psum x1, blocking collectives, local(): squares = lax.psum(square_part, 'kv')  13.6 us
    all_gather x1, blocking collectives, local(): lax.all_gather((share * rscale[:, None]).astype(jnp.bfloat16), 'kv')  13.6 us
    all_gather x1, blocking collectives, local(): every = lax.all_gather(shard_rest[None], 'kv', axis=0, tiled=True)  13.2 us
    reduce_scatter x1, waiting for transfers between devices, local(): lax.psum_scatter(partial_value, 'kv', scatter_dimension=1, tiled=True)  7.6 us
    psum x1, blocking collectives, local(): lax.psum(part_out.astype(jnp.bfloat16), 'tp')  3.96 us
    unnamed x29, local copies, waits for them, and re-layouts  3.44 us
  transfers between devices with their start and end apart: 2, of which 2 were waited for; matrix products, arithmetic and copies ran while one was open for 5% of the time, Pallas kernels for 0%

profile of v1, /device:TPU:0, one launch (start us, length us, event | category | flops | bytes accessed | tf_op | source)
XLA Modules:
  0.0 115.4 jit_solution(5456594110192393012)
XLA Ops:
  7.3 1.3 %copy-done = bf16[512,1536]{1,0:T(8,128)(2,1)S(1)} copy-done((bf16[512,1536]{1,0:T(8,128)(2,1)S(1)}, bf16[512,1536]{1,0:T(8,128)(2,1)}, u32[]{:S(2)}) %copy-start) | copy-done | bytes 1572888
  8.6 1.1 fusion.70
  9.8 0.3 fusion.68
  10.4 0.8 copy-done.6
  11.6 0.8 pad_maximum_fusion
  14.7 13.6 %psum.21 = f32[16]{0:T(128)S(1)} all-reduce(f32[16]{0:T(128)S(1)} %fusion.52), channel_id=1, replica_groups=mesh['dp'=4,'kv'=4,'tp'=2] {'kv'}, use_global_device_ids=true, to_apply=%region_2.0 | all-reduce | flops 16 | bytes 128 | tf_op jit(solution)/shard_map/psum | solution.py:60
  28.4 7.6 %reduce-scatter.2.cloned.1.call-done = f32[16,1536]{1,0:T(8,128)} async-done(((f32[16,6144]{1,0:T(8,128)}), f32[16,1536]{1,0:T(8,128)}) %reduce-scatter.2.cloned.1.call-update) | async-done | bytes 98320 | tf_op jit(solution)/shard_map/reduce_scatter | solution.py:61
  36.0 1.0 multiply_convert_fusion
  37.0 13.6 %all-gather = bf16[64,1536]{1,0:T(8,128)(2,1)S(1)} all-gather(bf16[16,1536]{1,0:T(8,128)(2,1)S(1)} %multiply_convert_fusion), channel_id=2, replica_groups=mesh['dp'=4,'kv'=4,'tp'=2] {'kv'}, dimensions={0}, use_global_device_ids=true | all-gather | bytes 245760 | tf_op jit(solution)/shard_map/all_gather | solution.py:64
  50.7 0.8 reshape.378
  51.6 0.9 fusion.80
  52.7 0.5 fusion.32
  53.2 0.3 fusion.31
  53.5 13.2 %all-gather.2 = f32[4,12,16]{2,1,0:T(8,128)S(1)} all-gather(f32[1,12,16]{2,1,0:T(8,128)S(1)} %bitcast.112), channel_id=3, replica_groups=mesh['dp'=4,'kv'=4,'tp'=2] {'kv'}, dimensions={0}, use_global_device_ids=true | all-gather | bytes 3840 | tf_op jit(solution)/shard_map/all_gather | solution.py:91
  66.9 0.9 fusion.13
  67.8 0.5 copy-done.2
  68.3 1.0 fusion.14
  69.3 1.8 %bitcast_select_fusion.1 = bf16[1,512,12,128]{3,1,2,0:T(8,128)(2,1)} fusion(bf16[1,512,12,128]{3,1,2,0:T(8,128)(2,1)S(1)} %copy-done.1, pred[512]{0:T(512)(128)(4,1)S(1)} %compare_and_fusion, bf16[1,16,1,12,128]{4,3,2,1,0:T(8,128)(2,1)S(1)} %get-tuple-element.4, s32[512]{0:T(512)S(1)} %fusion.73), kind=kOutput, calls=%fused_computation.3 | convolution fusion | flops 26746880 | bytes 3197440 | tf_op jit(solution)/shard_map/scp,sphd->schd/dot_general | solution.py:118
  71.1 1.8 %bitcast_select_fusion = bf16[1,512,12,128]{3,1,2,0:T(8,128)(2,1)} fusion(bf16[1,512,12,128]{3,1,2,0:T(8,128)(2,1)S(1)} %copy-done.3, pred[512]{0:T(512)(128)(4,1)S(1)} %compare_and_fusion, bf16[1,16,1,12,128]{4,3,2,1,0:T(8,128)(2,1)S(1)} %get-tuple-element.3, s32[512]{0:T(512)S(1)} %fusion.73), kind=kOutput, calls=%fused_computation.2 | convolution fusion | flops 26746880 | bytes 3197440 | tf_op jit(solution)/shard_map/scp,sphd->schd/dot_general | solution.py:121
  73.1 0.7 copy.45
  73.8 28.5 %all-reduce.2.cloned.1.call-done = f32[1,16,12,128]{3,1,2,0:T(8,128)} async-done(((f32[1,16,12,128]{3,1,2,0:T(8,128)}), f32[1,16,12,128]{3,1,2,0:T(8,128)}) %all-reduce.2.cloned.1.call-update) | async-done | bytes 98320 | tf_op jit(solution)/shard_map/psum | solution.py:105
  102.3 1.1 fusion.17
  103.5 1.1 convolution_convert_fusion.2
  104.6 4.0 %psum.23 = bf16[1,16,512]{2,1,0:T(8,128)(2,1)} all-reduce(bf16[1,16,512]{2,1,0:T(8,128)(2,1)S(1)} %bitcast.111), channel_id=1, replica_groups=mesh['dp'=4,'kv'=4,'tp'=2] {'tp'}, use_global_device_ids=true, to_apply=%region_7.8 | all-reduce | flops 8192 | bytes 32768 | tf_op jit(solution)/shard_map/psum | solution.py:112
  (50 shorter events, 2.6 us)
Async XLA Ops:
  7.2 1.4 %copy-start = (bf16[512,1536]{1,0:T(8,128)(2,1)S(1)}, bf16[512,1536]{1,0:T(8,128)(2,1)}, u32[]{:S(2)}) copy-start(bf16[512,1536]{1,0:T(8,128)(2,1)} %param.15) | copy-start | bytes 4718596
  7.2 2.5 %copy-start.8 = (bf16[1,16,512]{2,1,0:T(8,128)(2,1)S(1)}, bf16[1,16,512]{2,1,0:T(8,128)(2,1)}, u32[]{:S(2)}) copy-start(bf16[1,16,512]{2,1,0:T(8,128)(2,1)} %param.13) | copy-start | bytes 49156
  7.2 2.5 %copy-start.11 = (f32[512]{0:T(512)S(1)}, f32[512]{0:T(512)}, u32[]{:S(2)}) copy-start(f32[512]{0:T(512)} %param.14) | copy-start | bytes 6148
  7.2 2.5 %copy-start.4 = (bf16[512,1536]{1,0:T(8,128)(2,1)S(1)}, bf16[512,1536]{1,0:T(8,128)(2,1)}, u32[]{:S(2)}) copy-start(bf16[512,1536]{1,0:T(8,128)(2,1)} %param.16) | copy-start | bytes 4718596
  7.2 28.8 %reduce-scatter.2.cloned.1.call-start = ((), (), s32[]{:S(2)}) async-start(), calls=%async_computation.1 | async-start | bytes 491520 | tf_op jit(solution)/shard_map/reduce_scatter | solution.py:61
  8.6 1.6 %copy-start.5 = (bf16[512,1536]{1,0:T(8,128)(2,1)S(1)}, bf16[512,1536]{1,0:T(8,128)(2,1)}, u32[]{:S(2)}) copy-start(bf16[512,1536]{1,0:T(8,128)(2,1)} %param.17) | copy-start | bytes 4718596
  9.8 1.5 %copy-start.6 = (bf16[512,1536]{1,0:T(8,128)(2,1)S(1)}, bf16[512,1536]{1,0:T(8,128)(2,1)}, u32[]{:S(2)}) copy-start(bf16[512,1536]{1,0:T(8,128)(2,1)} %param.18) | copy-start | bytes 4718596
  11.3 1.2 %copy-start.13 = (s32[1,16]{1,0:T(1,128)S(1)}, s32[1,16]{1,0:T(1,128)}, u32[]{:S(2)}) copy-start(s32[1,16]{1,0:T(1,128)} %param.25) | copy-start | bytes 196
  11.6 40.9 %copy-start.12 = (f32[12]{0:T(128)S(1)}, f32[12]{0:T(128)}, u32[]{:S(2)}) copy-start(f32[12]{0:T(128)} %param.20) | copy-start | bytes 148
  11.6 41.1 %copy-start.1 = (bf16[1,512,12,128]{3,1,2,0:T(8,128)(2,1)S(1)}, bf16[1,512,12,128]{3,1,2,0:T(8,128)(2,1)}, u32[]{:S(2)}) copy-start(bf16[1,512,12,128]{3,1,2,0:T(8,128)(2,1)} %param.21) | copy-start | bytes 4718596
  12.4 90.0 %all-reduce.2.cloned.1.call-start = ((), (), s32[]{:S(2)}) async-start(), calls=%async_computation.2 | async-start | bytes 196608 | tf_op jit(solution)/shard_map/psum | solution.py:105
  52.7 15.1 %copy-start.9 = (f32[12,16,16]{1,2,0:T(8,128)}, f32[12,16,16]{1,2,0:T(8,128)S(1)}, u32[]{:S(2)}) copy-start(f32[12,16,16]{1,2,0:T(8,128)S(1)} %get-tuple-element.11) | copy-start | bytes 36868
  66.9 1.4 %copy-start.2 = (bf16[1,512,12,128]{3,1,2,0:T(8,128)(2,1)S(1)}, bf16[1,512,12,128]{3,1,2,0:T(8,128)(2,1)}, u32[]{:S(2)}) copy-start(bf16[1,512,12,128]{3,1,2,0:T(8,128)(2,1)} %param.22) | copy-start | bytes 4718596
  69.3 1.8 %copy-start.3 = (bf16[1,512,12,128]{3,1,2,0:T(8,128)(2,1)S(1)}, bf16[1,512,12,128]{3,1,2,0:T(8,128)(2,1)}, u32[]{:S(2)}) copy-start(bf16[1,512,12,128]{3,1,2,0:T(8,128)(2,1)} %param.22) | copy-start | bytes 4718596
  71.1 1.8 %copy-start.10 = (f32[12,16,16]{1,2,0:T(8,128)S(1)}, f32[12,16,16]{1,2,0:T(8,128)}, u32[]{:S(2)}) copy-start(f32[12,16,16]{1,2,0:T(8,128)} %copy-done.9) | copy-start | bytes 36868
  72.9 30.6 %copy-start.7 = (bf16[1536,512]{1,0:T(8,128)(2,1)S(1)}, bf16[1536,512]{1,0:T(8,128)(2,1)}, u32[]{:S(2)}) copy-start(bf16[1536,512]{1,0:T(8,128)(2,1)} %param.19) | copy-start | bytes 4718596
Sparse Core Ops, SparseCore 0:
  12.5 23.4 reduce-scatter.1
  69.4 32.8 all-reduce.1
